TPU v7x, 1024 devices: a whole 4x8x16 slice. The times are simulated.
1024 devices in a mesh: kv: 256 (over z, y, core), tp: 4 (over x).
Axes of the slice: x: 4, y: 8, z: 16, core: 2. Of those that a mesh axis runs over, the one named last changes fastest.
Arguments:
- hidden_rows: bfloat16 [98304, 2048], P('kv'), may hold values from -6 to 6
- proj_query: bfloat16 [2048, 2048], P(None, 'tp'), may hold values from -0.125 to 0.125
- proj_key: bfloat16 [2048, 256], P(None, 'tp'), may hold values from -0.125 to 0.125
- proj_value: bfloat16 [2048, 256], P(None, 'tp'), may hold values from -0.125 to 0.125
- proj_output: bfloat16 [2048, 2048], P('tp'), may hold values from -0.125 to 0.125
- head_scale: float32 [32], P('tp'), may hold values from 0.25 to 96
- hot_blocks: int32 [16], replicated, may hold values from 0 to 3071, as said below
- chosen_blocks: int32 [1536, 16], P('kv'), may hold values from 0 to 27, as said below
Outputs:
- layer_out: bfloat16 [98304, 2048], P('kv', 'tp')
Inputs may be any that keep to these rules, and one draw needn't show every extreme that they name: `hot_blocks`: 16 different key-block numbers; no device's 12 key blocks hold more than 2 of them, and in every draw some device holds exactly 2. `chosen_blocks`: each row's 16 codes name different key blocks; among them are the key blocks that cover the positions of query block b; no code of 12 or more names a block on the query block's own device.
All inputs are finite; a program needn't handle non-finite values.
Results may differ from a plain program's by a relative error of at most 0.01.
The roundings to bfloat16 on the way count: a program that leaves them out, or rounds other values in their place, can miss the bound.
Values may be sent and summed in bfloat16 or wider, within the bound.
A program may use at most 32 MiB of HBM per device.

v0:
```python
import jax
import jax.numpy as jnp
from jax import lax
from jax.sharding import Mesh
from jax.sharding import PartitionSpec as P

HD = 64
KB = 32
QB = 64
NSEL = 16
NHOT = 16
HOT_MOST = 2
KV = ("kv_0", "kv_1", "kv_2")


def laid_out(parts, dim):
    parts = jnp.moveaxis(parts, 0, dim)
    lengths = parts.shape
    return parts.reshape(*lengths[:dim], lengths[dim] * lengths[dim + 1], *lengths[dim + 2 :])


def stacked_from(array, axes, order):
    parts = array[None]
    for k in order:
        parts = lax.all_gather(parts, axes[k], axis=0, tiled=True)
    carried = [lax.axis_size(axes[k]) for k in reversed(order)]
    parts = parts.reshape(*carried, *array.shape)
    turned = sorted(range(len(order)), key=lambda place: order[len(order) - 1 - place])
    return parts.transpose(*turned, *range(len(order), parts.ndim)).reshape(-1, *array.shape)


def whole_of(array, axes, order, dim):
    return laid_out(stacked_from(array, axes, order), dim)


def cut_along(array, dim, size):
    lengths = array.shape
    parts = array.reshape(*lengths[:dim], size, lengths[dim] // size, *lengths[dim + 1 :])
    return jnp.moveaxis(parts, dim, 0)


def sent_and_summed(array, axis, dim):
    parts = cut_along(array, dim, lax.axis_size(axis))
    arrived = lax.all_to_all(parts, axis, split_axis=0, concat_axis=0, tiled=True)
    return arrived.astype(jnp.float32).sum(axis=0)


def local(
    hidden_rows,
    proj_query,
    proj_key,
    proj_value,
    proj_output,
    head_scale,
    hot_blocks,
    chosen_blocks,
):
    device = lax.axis_index(KV)
    tok_rows = hidden_rows.shape[0]
    own_blocks = tok_rows // KB
    kv_heads = proj_key.shape[1] // HD
    head_count = proj_query.shape[1] // HD
    group_size = head_count // kv_heads
    width = 2 * kv_heads * HD
    queries = jnp.dot(hidden_rows, proj_query, preferred_element_type=jnp.float32).astype(
        jnp.bfloat16
    )
    both_proj = jnp.concatenate([proj_key, proj_value], axis=1)
    packed = jnp.dot(hidden_rows, both_proj, preferred_element_type=jnp.float32).astype(
        jnp.bfloat16
    )
    packed = packed.reshape(own_blocks, KB, width)
    owners = hot_blocks // own_blocks
    offsets = hot_blocks - owners * own_blocks
    is_mine = owners == device
    selector = (offsets[:, None] == jnp.arange(own_blocks, dtype=jnp.int32)[None, :]) & is_mine[
        :, None
    ]
    hot_range = jnp.arange(NHOT, dtype=jnp.int32)
    before = hot_range[None, :] < hot_range[:, None]
    ranking = jnp.sum(((owners[None, :] == owners[:, None]) & before).astype(jnp.int32), axis=1)
    slot_of = owners * HOT_MOST + ranking
    slot_mask = (ranking[None, :] == jnp.arange(HOT_MOST, dtype=jnp.int32)[:, None]) & is_mine[
        None, :
    ]
    slot_pick = jnp.dot(
        slot_mask.astype(jnp.bfloat16),
        selector.astype(jnp.bfloat16),
        preferred_element_type=jnp.float32,
    ).astype(jnp.bfloat16)
    packed_slots = jnp.einsum(
        "sn,nkw->skw", slot_pick, packed, preferred_element_type=jnp.float32
    ).astype(jnp.bfloat16)
    piece = whole_of(packed_slots, KV, (0, 1, 2), 0)
    piece_rows = piece.shape[0]
    match = slot_of[:, None] == jnp.arange(piece_rows, dtype=jnp.int32)[None, :]
    added = jnp.einsum(
        "hm,mkw->hkw", match.astype(jnp.bfloat16), piece, preferred_element_type=jnp.float32
    ).astype(jnp.bfloat16)
    pool = jnp.concatenate([packed, added], axis=0)
    hot_match = (
        chosen_blocks[:, :, None] - own_blocks == jnp.arange(NHOT, dtype=jnp.int32)[None, None, :]
    )
    hot_global = jnp.sum(jnp.where(hot_match, hot_blocks[None, None, :], 0), axis=2)
    global_ids = jnp.where(
        chosen_blocks < own_blocks, device * own_blocks + chosen_blocks, hot_global
    )
    query_blocks = tok_rows // QB
    gathered = jnp.take(pool, chosen_blocks, axis=0).reshape(
        query_blocks, NSEL * KB, 2 * kv_heads, HD
    )
    key_rows = gathered[:, :, :kv_heads]
    value_rows = gathered[:, :, kv_heads:]
    grouped_query = queries.reshape(query_blocks, QB, kv_heads, group_size, HD)
    scores = jnp.einsum(
        "bqcgd,blcd->bcgql", grouped_query, key_rows, preferred_element_type=jnp.float32
    ) * HD ** (-0.5)
    scores = scores * head_scale.reshape(kv_heads, group_size)[None, :, :, None, None]
    query_pos = device * tok_rows + jnp.arange(tok_rows, dtype=jnp.int32).reshape(query_blocks, QB)
    key_pos = global_ids[:, :, None] * KB + jnp.arange(KB, dtype=jnp.int32)[None, None, :]
    key_pos = key_pos.reshape(query_blocks, NSEL * KB)
    visible = key_pos[:, None, :] <= query_pos[:, :, None]
    scores = jnp.where(visible[:, None, None], scores, -jnp.inf)
    row_max = jnp.max(scores, axis=-1, keepdims=True)
    lifted = jnp.exp(scores - row_max)
    weights = (lifted / jnp.sum(lifted, axis=-1, keepdims=True)).astype(jnp.bfloat16)
    attended = jnp.einsum(
        "bcgql,blcd->bqcgd", weights, value_rows, preferred_element_type=jnp.float32
    ).astype(jnp.bfloat16)
    attended = attended.reshape(tok_rows, head_count * HD)
    partial_value = jnp.dot(attended, proj_output, preferred_element_type=jnp.float32)
    return sent_and_summed(partial_value.astype(jnp.bfloat16), "tp", 1).astype(jnp.bfloat16)


def solution(mesh):
    finer = Mesh(mesh.devices.reshape(16, 8, 2, mesh.shape["tp"]), ("kv_0", "kv_1", "kv_2", "tp"))
    placed = (
        P(KV, None),
        P(None, "tp"),
        P(None, "tp"),
        P(None, "tp"),
        P("tp", None),
        P("tp"),
        P(),
        P(KV, None),
    )
    return jax.shard_map(local, mesh=finer, in_specs=placed, out_specs=P(KV, "tp"), check_vma=False)
```

profile of v0, /device:TPU:1, one launch (start us, length us, event | category | flops | bytes accessed | tf_op | source)
XLA Modules:
  0.0 193.0 jit_solution(18128688554050870845)
XLA Ops:
  6.5 0.0 copy-start
  6.5 0.0 copy-start.3
  6.5 0.0 copy-start.2
  6.5 0.0 all-gather.4.cloned.1.call-start
  6.6 0.8 broadcast_compare_fusion.1
  7.4 0.2 convert_reduce_fusion
  7.6 0.7 multiply_add_fusion
  8.2 2.2 %fusion.11 = bf16[384,128]{0,1:T(8,128)(2,1)S(1)} fusion(bf16[384,2048]{1,0:T(8,128)(2,1)} %param.8, bf16[2048,64]{0,1:T(8,128)(2,1)} %param.11, bf16[2048,64]{0,1:T(8,128)(2,1)} %param.10), kind=kOutput, calls=%fused_computation.17 | convolution fusion | flops 202424320 | bytes 2195456 | tf_op jit(solution)/shard_map/dot_general | solution.py:69
  10.4 0.1 copy.50
  10.5 0.3 convolution_convert_fusion.4
  10.9 39.8 %all-gather = bf16[32,32,128]{2,1,0:T(8,128)(2,1)} all-gather(bf16[2,32,128]{2,1,0:T(8,128)(2,1)S(1)} %copy.52), channel_id=2, replica_groups=mesh['kv_0'=16,'kv_1'=8,'kv_2'=2,'tp'=4] {'kv_0'}, dimensions={0}, use_global_device_ids=true | all-gather | bytes 278528 | tf_op jit(solution)/shard_map/all_gather | solution.py:25
  50.7 0.0 all-gather.4.cloned.1.call-update
  50.7 0.0 all-gather.6.cloned.1.call-start
  50.7 44.6 %all-gather.4.cloned.1.call-done = bf16[128,2,32,128]{3,2,1,0:T(8,128)(2,1)} async-done(((bf16[16,2,32,128]{3,2,1,0:T(8,128)(2,1)}), bf16[128,2,32,128]{3,2,1,0:T(8,128)(2,1)}) %all-gather.4.cloned.1.call-update) | async-done | bytes 2097168 | tf_op jit(solution)/shard_map/all_gather | solution.py:25
  95.4 0.0 copy-start.4
  95.4 0.0 all-gather.6.cloned.1.call-update
  95.4 0.0 copy-done.2
  95.5 0.0 copy-done.3
  95.5 0.2 select_reduce_fusion
  95.7 0.1 reshape.108
  95.8 0.1 broadcast_in_dim.42
  95.9 0.1 broadcast_in_dim.43
  96.0 0.1 add.71
  96.1 0.1 add.72
  96.2 0.1 add.74
  96.2 3.0 %convolution_convert_fusion.1 = bf16[384,512]{1,0:T(8,128)(2,1)S(1)} fusion(bf16[384,2048]{1,0:T(8,128)(2,1)} %param.8, bf16[2048,512]{1,0:T(8,128)(2,1)} %param.9), kind=kOutput, calls=%fused_computation.14 | convolution fusion | flops 805502976 | bytes 4063232 | tf_op jit(solution)/shard_map/dot_general | solution.py:65
  99.3 1.3 reshape.102
  100.6 0.0 copy-done.4
  100.6 0.2 broadcast_compare_fusion
  100.8 30.4 %all-gather.6.cloned.1.call-done = bf16[256,2,32,128]{3,2,1,0:T(8,128)(2,1)} async-done(((bf16[128,2,32,128]{3,2,1,0:T(8,128)(2,1)}), bf16[256,2,32,128]{3,2,1,0:T(8,128)(2,1)}) %all-gather.6.cloned.1.call-update) | async-done | bytes 4194320 | tf_op jit(solution)/shard_map/all_gather | solution.py:25
  131.3 6.6 %copy.53 = bf16[16,8,2,2,32,128]{5,3,2,1,0,4:T(2,128)(2,1)S(1)} copy(bf16[16,8,2,2,32,128]{5,4,3,0,1,2:T(8,128)(2,1)} %bitcast.91) | data formatting | bytes 8388608 | tf_op jit(solution)/shard_map/transpose | solution.py:29
  137.9 0.7 convolution_convert_fusion.2
  138.6 0.1 pad_maximum_fusion
  138.7 0.0 copy-start.1
  138.7 0.1 copy.55
  138.8 1.6 gather_fusion
  140.4 3.9 %gather.7 = bf16[6,512,2,64]{3,2,1,0:T(2,128)(2,1)} reshape(bf16[96,32,128]{2,1,0:T(8,128)(2,1)} %gather_fusion) | data formatting | bytes 1572864 | tf_op jit(solution)/shard_map/jit(_take)/gather | solution.py:109
  144.3 4.7 %copy.56 = bf16[6,512,2,64]{1,3,0,2:T(8,128)(2,1)} copy(bf16[6,512,2,64]{3,2,1,0:T(2,128)(2,1)} %gather.7) | data formatting | bytes 1572864 | tf_op jit(solution)/shard_map/jit(_take)/gather | solution.py:109
  149.0 1.2 broadcast_select_fusion
  150.2 0.0 copy-done.1
  150.2 1.1 fusion.1
  151.3 1.9 fusion
  153.2 3.5 %fusion.8 = bf16[6,64,1,8,64]{1,4,3,0,2:T(8,128)(2,1)} fusion(f32[6,8,64]{2,1,0:T(8,128)S(1)} %fusion, f32[6,8,64]{2,1,0:T(8,128)S(1)} %get-tuple-element.11, f32[8]{0:T(128)S(1)} %broadcast_multiply_fusion, f32[6,512,64,8]{1,2,3,0:T(8,128)S(1)} %get-tuple-element.12, pred[6,64,512]{2,1,0:T(8,128)(4,1)S(1)} %broadcast_compare_fusion, ...), kind=kOutput, calls=%fused_computation.13 | convolution fusion | flops 209387520 | bytes 7324160 | tf_op jit(solution)/shard_map/bcgql,blcd->bqcgd/dot_general | solution.py:127
  156.7 1.6 copy.58
  158.3 0.5 reshape.104
  158.8 0.0 copy-done
  158.8 1.0 convolution_convert_fusion
  159.8 0.1 copy.70
  159.9 23.7 %all_to_all.5 = bf16[4,384,512]{2,1,0:T(8,128)(2,1)} all-to-all(bf16[4,384,512]{2,1,0:T(8,128)(2,1)S(1)} %bitcast.90), channel_id=1, replica_groups=mesh['kv_0'=16,'kv_1'=8,'kv_2'=2,'tp'=4] {'tp'}, dimensions={0} | all-to-all | bytes 3145728 | tf_op jit(solution)/shard_map/all_to_all | solution.py:44
  183.6 2.5 %reduce_sum.42 = bf16[384,512]{1,0:T(8,128)(2,1)} reduce(bf16[4,384,512]{2,1,0:T(8,128)(2,1)} %all_to_all.5, bf16[]{:T(256)} %constant.67.clone.1), dimensions={0}, to_apply=%region_4.5 | reduce | flops 589824 | bytes 1966082 | tf_op jit(solution)/shard_map/reduce_sum | solution.py:45
  (10 shorter events, 0.1 us)
Async XLA Ops:
  6.5 152.2 %copy-start = (bf16[512,2048]{1,0:T(8,128)(2,1)S(1)}, bf16[512,2048]{1,0:T(8,128)(2,1)}, u32[]{:S(2)}) copy-start(bf16[512,2048]{1,0:T(8,128)(2,1)} %param.12) | copy-start | bytes 6291460
  6.5 88.9 %copy-start.3 = (s32[16]{0:T(128)S(1)}, s32[16]{0:T(128)}, u32[]{:S(2)}) copy-start(s32[16]{0:T(128)} %param.14) | copy-start | bytes 196
  6.5 88.9 %copy-start.2 = (s32[6,16]{1,0:T(8,128)S(1)}, s32[6,16]{1,0:T(8,128)}, u32[]{:S(2)}) copy-start(s32[6,16]{1,0:T(8,128)} %param.15) | copy-start | bytes 1156
  6.5 88.8 %all-gather.4.cloned.1.call-start = ((), (), s32[]{:S(2)}) async-start(), calls=%async_computation.1 | async-start | bytes 2359296 | tf_op jit(solution)/shard_map/all_gather | solution.py:25
  50.7 80.6 %all-gather.6.cloned.1.call-start = ((), (), s32[]{:S(2)}) async-start(), calls=%async_computation.2 | async-start | bytes 6291456 | tf_op jit(solution)/shard_map/all_gather | solution.py:25
  95.4 5.3 %copy-start.4 = (f32[8]{0:T(128)S(1)}, f32[8]{0:T(128)}, u32[]{:S(2)}) copy-start(f32[8]{0:T(128)} %param.13) | copy-start | bytes 100
  138.7 11.5 %copy-start.1 = (bf16[6,64,8,64]{3,2,1,0:T(8,128)(2,1)S(1)}, bf16[6,64,8,64]{3,2,1,0:T(8,128)(2,1)}, u32[]{:S(2)}) copy-start(bf16[6,64,8,64]{3,2,1,0:T(8,128)(2,1)} %reshape.102) | copy-start | bytes 1179652
Sparse Core Ops, SparseCore 0:
  50.8 44.4 all-gather.3
  98.0 33.1 all-gather.5
where the time goes:
time: 194 us; the launch traced here: 193 us
  waiting for transfers between devices  75.1 us (39%)
  blocking collectives  63.5 us (33%)
  local copies, waits for them, and re-layouts  21 us (11%)
  between operations  13.6 us (7%)
  matrix products  11.9 us (6%)
  other arithmetic  7.82 us (4%)
    all_gather x2, waiting for transfers between devices, stacked_from(): parts = lax.all_gather(parts, axes[k], axis=0, tiled=True)  75.1 us
    all_gather x1, blocking collectives, stacked_from(): parts = lax.all_gather(parts, axes[k], axis=0, tiled=True)  39.8 us
    all_to_all x1, blocking collectives, sent_and_summed(): lax.all_to_all(parts, axis, split_axis=0, concat_axis=0, tiled=True)  23.7 us
    gather x3, local copies, waits for them, and re-layouts, local(): jnp.take(pool, chosen_blocks, axis=0)  10.2 us
    transpose x1, local copies, waits for them, and re-layouts, stacked_from(): parts.transpose(*turned, *range(len(order), parts.ndim))  6.62 us
  transfers between devices with their start and end apart: 2, of which 2 were waited for; matrix products, arithmetic and copies ran while one was open for 3% of the time, Pallas kernels for 0%

commit v1 on v0

v1 whole, which is shorter than its diff:
```python
import functools

import jax
import jax.numpy as jnp
from jax import lax
from jax.experimental import pallas as pl
from jax.experimental.pallas import tpu as pltpu
from jax.sharding import Mesh
from jax.sharding import PartitionSpec as P

HD = 64
KB = 32
QB = 64
NSEL = 16
NHOT = 16
FAR = 1 << 30
F32 = jnp.float32
BF16 = jnp.bfloat16
MESH = pl.DeviceIdType.MESH


def outward(count):
    return sorted(range(1, count), key=lambda k: -min(k, count - k))


def row_order(row):
    return sorted(range(1, row), key=lambda k: -min(k, row - k))


def kernel(
    dims,
    x_hbm,
    wq_hbm,
    wk_hbm,
    wv_hbm,
    wo_hbm,
    scale_hbm,
    hot_hbm,
    codes_hbm,
    out_ref,
    x,
    wq,
    wkv,
    wo,
    scale,
    hot,
    codes,
    local_kv,
    kv_all,
    vk_all,
    q_even,
    q_odd,
    bias,
    give,
    got,
    part,
    around,
    scores,
    weights,
    opp,
    via,
    side,
    arrived,
    own,
    in_sem,
    hot_send,
    hot_recv,
    tp_send,
    tp_recv,
):
    nz, ny, nc, ntp = dims
    row = ny * nc
    z = lax.axis_index("z")
    r = lax.axis_index("y") * nc + lax.axis_index("c")
    s = lax.axis_index("tp")
    tokens, width = x.shape
    blocks = tokens // QB
    own_blocks = tokens // KB
    keys = kv_all.shape[0]
    base = (z * row + r) * tokens

    def in_row(k):
        t = lax.rem(r + k, row)
        return {"y": t // nc, "c": lax.rem(t, nc)}

    def in_z(k):
        return {"z": lax.rem(z + k, nz)}

    right = {"tp": lax.rem(s + 1, ntp)}
    left = {"tp": lax.rem(s + ntp - 1, ntp)}

    def load(i, src, dst):
        c = pltpu.make_async_copy(src, dst, in_sem.at[i])
        c.start()
        return c

    hot_in = load(0, hot_hbm, hot)
    kv_in = [load(1, x_hbm, x)]
    for i, src in enumerate((wk_hbm, wv_hbm, wv_hbm, wk_hbm)):
        kv_in.append(load(2 + i, src, wkv.at[pl.ds(HD * i, HD)]))
    q_in = load(6, wq_hbm, wq)
    codes_in = load(7, codes_hbm, codes)
    scale_in = load(8, scale_hbm, scale)
    wo_in = load(9, wo_hbm, wo)

    barrier = pltpu.get_barrier_semaphore()
    for k in outward(nz):
        pl.semaphore_signal(barrier, inc=1, device_id=in_z(k), device_id_type=MESH)
    for k in range(1, row):
        pl.semaphore_signal(barrier, inc=1, device_id=in_row(k), device_id_type=MESH)
    for peer in (left, right):
        pl.semaphore_signal(barrier, inc=1, device_id=peer, device_id_type=MESH)

    for c in kv_in:
        c.wait()
    both = lax.dot_general(
        x[...], wkv[...], (((1,), (1,)), ((), ())), preferred_element_type=F32
    ).astype(BF16)
    packed = both[:, : 2 * HD]
    local_kv[...] = packed.reshape(own_blocks, KB, 2 * HD)
    kv_all[pl.ds(0, tokens)] = packed
    vk_all[pl.ds(0, tokens)] = both[:, 2 * HD :]
    hot_in.wait()
    for j in range(NHOT):
        owner = hot[j] // own_blocks
        mine = owner == z * row + r
        block = local_kv[hot[j] - owner * own_blocks].astype(F32)
        give[j] = jnp.where(mine, block, 0.0).astype(BF16)

    pl.semaphore_wait(barrier, nz - 1 + row - 1 + 2)

    def first(k):
        return pltpu.make_async_remote_copy(
            give.at[lax.rem(r + k, row)], got.at[0, k], hot_send.at[0, k], hot_recv.at[0, k],
            device_id=in_row(k), device_id_type=MESH,
        )

    def second(k):
        return pltpu.make_async_remote_copy(
            part, got.at[1, k], hot_send.at[1, k], hot_recv.at[1, k],
            device_id=in_z(k), device_id_type=MESH,
        )

    def third(k):
        rows = pl.ds(pl.multiple_of(tokens + r * KB, KB), KB)
        return pltpu.make_async_remote_copy(
            around, kv_all.at[rows], hot_send.at[2, k], hot_recv.at[2, k],
            device_id=in_row(k), device_id_type=MESH,
        )

    for k in row_order(row):
        first(k).start()

    q_in.wait()
    pairs = wq.shape[1] // (2 * HD)
    low = lax.broadcasted_iota(jnp.int32, (QB, 2 * HD), 1) < HD
    queries = jnp.dot(x[...], wq[...], preferred_element_type=F32)
    for b in range(blocks):
        for i in range(pairs):
            tile = queries[b * QB : (b + 1) * QB, i * 2 * HD : (i + 1) * 2 * HD]
            q_even[b, pl.ds(i * QB, QB)] = jnp.where(low, tile, 0.0).astype(BF16)
            q_odd[b, pl.ds(i * QB, QB)] = jnp.where(low, 0.0, tile).astype(BF16)

    total = give[r].astype(F32)
    for k in range(1, row):
        first(k).wait_recv()
        total = total + got[0, k].astype(F32)
    part[...] = total.astype(BF16)
    for k in outward(nz):
        second(k).start()

    codes_in.wait()
    scale_in.wait()
    lane = lax.broadcasted_iota(jnp.int32, (8, keys), 1)
    number = lane >> 5
    key_pos = base + lane
    for j in range(NHOT):
        key_pos = jnp.where(number == own_blocks + j, hot[j] * KB + (lane & (KB - 1)), key_pos)
    for b in range(blocks):
        chosen = number == codes[b, 0]
        for e in range(1, NSEL):
            chosen = chosen | (number == codes[b, e])
        seen = jnp.where(chosen, key_pos, FAR)[0:1]
        query_pos = base + b * QB + lax.broadcasted_iota(jnp.int32, (QB, 1), 0)
        bias[b] = jnp.where(seen <= query_pos, 0.0, -jnp.inf)

    total = part[...].astype(F32)
    for k in range(1, nz):
        second(k).wait_recv()
        total = total + got[1, k].astype(F32)
    around[...] = total.astype(BF16)
    for k in row_order(row):
        third(k).start()
    kv_all[pl.ds(pl.multiple_of(tokens + r * KB, KB), KB)] = total.astype(BF16)
    wo_in.wait()
    for k in range(1, row):
        third(k).wait_recv()
    hot_rows = kv_all[pl.ds(tokens, NHOT * KB)].astype(F32)
    vk_all[pl.ds(tokens, NHOT * KB)] = pltpu.roll(hot_rows, HD, 1).astype(BF16)

    cols = wo.shape[1] // ntp
    half = cols // 2

    def copy(kind, c):
        src, dst, peer = (
            (opp.at[c, 0], via.at[c, 0], left),
            (opp.at[c, 1], via.at[c, 1], right),
            (side.at[c, 0, 1], arrived.at[c, 1, 1], left),
            (side.at[c, 1, 0], arrived.at[c, 0, 0], right),
            (side.at[c, 0, 0], arrived.at[c, 1, 0], left),
            (side.at[c, 1, 1], arrived.at[c, 0, 1], right),
        )[kind]
        return pltpu.make_async_remote_copy(
            src, dst, tp_send.at[kind, c], tp_recv.at[kind, c],
            device_id=peer, device_id_type=MESH,
        )

    def columns(shift):
        at = pl.multiple_of(lax.rem(s + shift, ntp) * cols, cols)
        return wo[:, pl.ds(at, cols)]

    def attend(b):
        outs = []
        for odd, q, rhs, val in ((0, q_even, kv_all, vk_all), (1, q_odd, vk_all, kv_all)):
            scores[odd] = lax.dot_general(
                q[b], rhs[...], (((1,), (1,)), ((), ())), preferred_element_type=F32
            )
            for i in range(pairs):
                factor = scale[2 * i + odd] * HD ** (-0.5)
                for p in range(2):
                    rows = pl.ds(i * QB + p * (QB // 2), QB // 2)
                    sc = scores[odd, rows] * factor + bias[b, pl.ds(p * (QB // 2), QB // 2)]
                    top = jnp.max(sc, axis=-1, keepdims=True)
                    lifted = jnp.exp(sc - top)
                    norm = 1.0 / jnp.sum(lifted, axis=-1, keepdims=True)
                    weights[odd, rows] = (lifted * norm).astype(BF16)
            outs.append(jnp.dot(weights[odd], val[...], preferred_element_type=F32))
        tiles = [
            jnp.where(low, outs[0][i * QB : (i + 1) * QB], outs[1][i * QB : (i + 1) * QB])
            for i in range(pairs)
        ]
        return jnp.concatenate(tiles, axis=1).astype(BF16)

    def produce(c):
        att = attend(c)
        far = jnp.dot(att, columns(2), preferred_element_type=F32).astype(BF16)
        opp[c, 0] = far[:, :half]
        opp[c, 1] = far[:, half:]
        copy(0, c).start()
        copy(1, c).start()
        to_left = jnp.dot(att, columns(ntp - 1), preferred_element_type=F32).astype(BF16)
        side[c, 0, 0] = to_left[:, :half]
        side[c, 0, 1] = to_left[:, half:]
        copy(2, c).start()
        to_right = jnp.dot(att, columns(1), preferred_element_type=F32).astype(BF16)
        side[c, 1, 0] = to_right[:, :half]
        side[c, 1, 1] = to_right[:, half:]
        copy(3, c).start()
        own[c] = jnp.dot(att, columns(0), preferred_element_type=F32).astype(BF16)

    def combine(c):
        for d in range(2):
            copy(d, c).wait_recv()
            side[c, d, d] = (side[c, d, d].astype(F32) + via[c, d].astype(F32)).astype(BF16)
            copy(4 + d, c).start()

    def finish(c):
        for kind in range(2, 6):
            copy(kind, c).wait_recv()
        rows = pl.ds(pl.multiple_of(c * QB, QB), QB)
        for h in range(2):
            part_sum = own[c, :, h * half : (h + 1) * half].astype(F32)
            part_sum = part_sum + arrived[c, 0, h].astype(F32) + arrived[c, 1, h].astype(F32)
            out_ref[rows, h * half : (h + 1) * half] = part_sum.astype(BF16)

    def step(c, carry):
        @pl.when(c < blocks)
        def _():
            produce(c)

        @pl.when((c >= 1) & (c <= blocks))
        def _():
            combine(c - 1)

        @pl.when(c >= 2)
        def _():
            finish(c - 2)

        return carry

    lax.fori_loop(0, blocks + 2, step, 0)

    for k in range(1, row):
        first(k).wait_send()
        third(k).wait_send()
    for k in range(1, nz):
        second(k).wait_send()
    for c in range(blocks):
        for kind in range(6):
            copy(kind, c).wait_send()


def local(
    dims,
    hidden_rows,
    proj_query,
    proj_key,
    proj_value,
    proj_output,
    head_scale,
    hot_blocks,
    chosen_blocks,
):
    nz, ny, nc, ntp = dims
    tokens, width = hidden_rows.shape
    head_cols = proj_query.shape[1]
    out_cols = proj_output.shape[1]
    cols = out_cols // ntp
    half = cols // 2
    blocks = tokens // QB
    keys = tokens + NHOT * KB
    stacked = head_cols // (2 * HD) * QB
    row = ny * nc
    anywhere = pl.BlockSpec(memory_space=pl.ANY)
    return pl.pallas_call(
        functools.partial(kernel, dims),
        out_shape=jax.ShapeDtypeStruct((tokens, cols), BF16),
        in_specs=[anywhere] * 8,
        out_specs=pl.BlockSpec(memory_space=pltpu.VMEM),
        scratch_shapes=[
            pltpu.VMEM((tokens, width), BF16),
            pltpu.VMEM((width, head_cols), BF16),
            pltpu.VMEM((4 * HD, width), BF16),
            pltpu.VMEM((head_cols, out_cols), BF16),
            pltpu.SMEM((head_cols // HD,), F32),
            pltpu.SMEM((NHOT,), jnp.int32),
            pltpu.SMEM((blocks, NSEL), jnp.int32),
            pltpu.VMEM((tokens // KB, KB, 2 * HD), BF16),
            pltpu.VMEM((keys, 2 * HD), BF16),
            pltpu.VMEM((keys, 2 * HD), BF16),
            pltpu.VMEM((blocks, stacked, 2 * HD), BF16),
            pltpu.VMEM((blocks, stacked, 2 * HD), BF16),
            pltpu.VMEM((blocks, QB, keys), F32),
            pltpu.VMEM((NHOT, KB, 2 * HD), BF16),
            pltpu.VMEM((2, NHOT, KB, 2 * HD), BF16),
            pltpu.VMEM((KB, 2 * HD), BF16),
            pltpu.VMEM((KB, 2 * HD), BF16),
            pltpu.VMEM((2, stacked, keys), F32),
            pltpu.VMEM((2, stacked, keys), BF16),
            pltpu.VMEM((blocks, 2, QB, half), BF16),
            pltpu.VMEM((blocks, 2, QB, half), BF16),
            pltpu.VMEM((blocks, 2, 2, QB, half), BF16),
            pltpu.VMEM((blocks, 2, 2, QB, half), BF16),
            pltpu.VMEM((blocks, QB, cols), BF16),
            pltpu.SemaphoreType.DMA((10,)),
            pltpu.SemaphoreType.DMA((3, NHOT)),
            pltpu.SemaphoreType.DMA((3, NHOT)),
            pltpu.SemaphoreType.DMA((6, blocks)),
            pltpu.SemaphoreType.DMA((6, blocks)),
        ],
        compiler_params=pltpu.CompilerParams(collective_id=0, has_side_effects=True),
    )(
        hidden_rows,
        proj_query,
        proj_key.T,
        proj_value.T,
        proj_output,
        head_scale,
        hot_blocks,
        chosen_blocks,
    )


def solution(mesh):
    ntp = mesh.shape["tp"]
    dims = (16, 8, 2, ntp)
    finer = Mesh(mesh.devices.reshape(dims), ("z", "y", "c", "tp"))
    kv = ("z", "y", "c")
    placed = (
        P(kv, None),
        P(None, "tp"),
        P(None, "tp"),
        P(None, "tp"),
        P("tp", None),
        P("tp"),
        P(),
        P(kv, None),
    )
    return jax.shard_map(
        functools.partial(local, dims),
        mesh=finer,
        in_specs=placed,
        out_specs=P(kv, "tp"),
        check_vma=False,
    )
```

time: 194 us -> 69.1 us (0.36)
  the two profiles are of different devices: /device:TPU:1 before, /device:TPU:8 now
where the time goes in v1:
time: 69.1 us; the launch traced here: 68.9 us
  Pallas kernels  67.1 us (97%)
  local copies, waits for them, and re-layouts  1.77 us (3%)
    pallas_call x1, Pallas kernels, local(): pl.pallas_call(functools.partial(kernel, dims), out_shape=jax.ShapeDtypeS...  67.1 us
    unnamed x1, local copies, waits for them, and re-layouts  1.77 us

profile of v1, /device:TPU:8, one launch (start us, length us, event | category | flops | bytes accessed | tf_op | source)
XLA Modules:
  0.0 68.9 jit_solution(13344111530579072907)
XLA Ops:
  0.0 67.1 %shard_map.82 = bf16[384,512]{1,0:T(8,128)(2,1)} custom-call(bf16[384,2048]{1,0:T(8,128)(2,1)} %x_hbm.1, bf16[2048,512]{1,0:T(8,128)(2,1)} %wq_hbm.1, bf16[64,2048]{1,0:T(8,128)(2,1)} %bitcast.2, bf16[64,2048]{1,0:T(8,128)(2,1)} %bitcast.3, bf16[512,2048]{1,0:T(8,128)(2,1)} %wo_hbm.1, f32[8]{0:T(128)} %scale_hbm.1, s32[16]{0:T(128)} %hot_hbm.1, ...), custom_call_target="tpu_custom_call" | custom-call | tf_op jit(solution)/shard_map/pallas_call | solution.py:325
  67.2 1.8 %copy.10 = bf16[384,512]{1,0:T(8,128)(2,1)} copy(bf16[384,512]{1,0:T(8,128)(2,1)} %shard_map.82) | data formatting | bytes 786432

commit v2 on v1

--- a/solution.py
+++ b/solution.py
@@ -14,13 +14,11 @@
 NSEL = 16
 NHOT = 16
 FAR = 1 << 30
+PIECES = 4
+LOG2E = 1.4426950408889634
 F32 = jnp.float32
 BF16 = jnp.bfloat16
 MESH = pl.DeviceIdType.MESH
-
-
-def outward(count):
-    return sorted(range(1, count), key=lambda k: -min(k, count - k))
 
 
 def row_order(row):
@@ -57,6 +55,12 @@
     around,
     scores,
     weights,
+    local_out,
+    local_top,
+    local_sum,
+    hot_sc,
+    hot_w,
+    attended,
     opp,
     via,
     side,
@@ -67,6 +71,7 @@
     hot_recv,
     tp_send,
     tp_recv,
+    aware,
 ):
     nz, ny, nc, ntp = dims
     row = ny * nc
@@ -95,31 +100,40 @@
         return c
 
     hot_in = load(0, hot_hbm, hot)
-    kv_in = [load(1, x_hbm, x)]
-    for i, src in enumerate((wk_hbm, wv_hbm, wv_hbm, wk_hbm)):
-        kv_in.append(load(2 + i, src, wkv.at[pl.ds(HD * i, HD)]))
-    q_in = load(6, wq_hbm, wq)
-    codes_in = load(7, codes_hbm, codes)
-    scale_in = load(8, scale_hbm, scale)
-    wo_in = load(9, wo_hbm, wo)
+    kv_in = [
+        load(1, wk_hbm, wkv.at[pl.ds(0, HD)]),
+        load(2, wv_hbm, wkv.at[pl.ds(HD, HD)]),
+    ]
+    slab = width // PIECES
+    slabs = [pl.ds(i * slab, slab) for i in range(PIECES)]
+    x_in = [load(3 + i, x_hbm.at[:, at], x.at[:, at]) for i, at in enumerate(slabs)]
 
     barrier = pltpu.get_barrier_semaphore()
-    for k in outward(nz):
-        pl.semaphore_signal(barrier, inc=1, device_id=in_z(k), device_id_type=MESH)
     for k in range(1, row):
         pl.semaphore_signal(barrier, inc=1, device_id=in_row(k), device_id_type=MESH)
     for peer in (left, right):
         pl.semaphore_signal(barrier, inc=1, device_id=peer, device_id_type=MESH)
 
+    def above(d, carry):
+        pl.semaphore_signal(barrier, inc=1, device_id={"z": d}, device_id_type=MESH)
+        return carry
+
+    lax.fori_loop(z + 1, nz, above, 0)
+
     for c in kv_in:
         c.wait()
-    both = lax.dot_general(
-        x[...], wkv[...], (((1,), (1,)), ((), ())), preferred_element_type=F32
-    ).astype(BF16)
-    packed = both[:, : 2 * HD]
+    both = jnp.zeros((tokens, 2 * HD), F32)
+    for c, at in zip(x_in, slabs):
+        c.wait()
+        both = both + lax.dot_general(
+            x[:, at], wkv[:, at], (((1,), (1,)), ((), ())), preferred_element_type=F32
+        )
+    q_in = load(3 + PIECES, wq_hbm, wq)
+    codes_in = load(4 + PIECES, codes_hbm, codes)
+    scale_in = load(5 + PIECES, scale_hbm, scale)
+    wo_in = load(6 + PIECES, wo_hbm, wo)
+    packed = both.astype(BF16)
     local_kv[...] = packed.reshape(own_blocks, KB, 2 * HD)
-    kv_all[pl.ds(0, tokens)] = packed
-    vk_all[pl.ds(0, tokens)] = both[:, 2 * HD :]
     hot_in.wait()
     for j in range(NHOT):
         owner = hot[j] // own_blocks
@@ -127,7 +141,7 @@
         block = local_kv[hot[j] - owner * own_blocks].astype(F32)
         give[j] = jnp.where(mine, block, 0.0).astype(BF16)
 
-    pl.semaphore_wait(barrier, nz - 1 + row - 1 + 2)
+    pl.semaphore_wait(barrier, row - 1 + 2 + z)
 
     def first(k):
         return pltpu.make_async_remote_copy(
@@ -148,8 +162,19 @@
             device_id=in_row(k), device_id_type=MESH,
         )
 
-    for k in row_order(row):
-        first(k).start()
+    def to_row(phase):
+        for k in row_order(row):
+            phase(k).start()
+
+    to_row(first)
+
+    def below(d, carry):
+        pl.semaphore_signal(aware.at[z], inc=1, device_id={"z": d}, device_id_type=MESH)
+        return carry
+
+    lax.fori_loop(0, z, below, 0)
+    kv_all[pl.ds(0, tokens)] = packed
+    vk_all[pl.ds(0, tokens)] = pltpu.roll(packed.astype(F32), HD, 1).astype(BF16)
 
     q_in.wait()
     pairs = wq.shape[1] // (2 * HD)
@@ -166,8 +191,12 @@
         first(k).wait_recv()
         total = total + got[0, k].astype(F32)
     part[...] = total.astype(BF16)
-    for k in outward(nz):
-        second(k).start()
+
+    def sink(d, carry):
+        second(lax.rem(d - z + nz, nz)).start()
+        return carry
+
+    lax.fori_loop(0, z, sink, 0)
 
     codes_in.wait()
     scale_in.wait()
@@ -184,13 +213,53 @@
         query_pos = base + b * QB + lax.broadcasted_iota(jnp.int32, (QB, 1), 0)
         bias[b] = jnp.where(seen <= query_pos, 0.0, -jnp.inf)
 
+    sides = ((0, q_even, kv_all, vk_all), (1, q_odd, vk_all, kv_all))
+    quarter = QB // 2
+    strips = [(i, p) for i in range(pairs) for p in range(2)]
+
+    def scored(b, odd, q, rhs, first_key, count):
+        at = pl.ds(first_key, count)
+        scores[odd, :, pl.ds(0, count)] = lax.dot_general(
+            q[b], rhs[at], (((1,), (1,)), ((), ())), preferred_element_type=F32
+        )
+
+    def strip(b, odd, i, p, first_key, count):
+        rows = pl.ds(i * QB + p * quarter, quarter)
+        factor = scale[2 * i + odd] * (HD ** (-0.5) * LOG2E)
+        seen = bias[b, pl.ds(p * quarter, quarter), pl.ds(first_key, count)]
+        return rows, scores[odd, rows, pl.ds(0, count)] * factor + seen
+
+    def own_keys(b, carry):
+        for odd, q, rhs, val in sides:
+            scored(b, odd, q, rhs, 0, tokens)
+            for i, p in strips:
+                rows, sc = strip(b, odd, i, p, 0, tokens)
+                top = jnp.max(sc, axis=-1, keepdims=True)
+                lifted = jnp.exp2(sc - top)
+                weights[odd, rows, pl.ds(0, tokens)] = lifted.astype(BF16)
+                local_top[b, odd, rows] = top
+                local_sum[b, odd, rows] = jnp.sum(lifted, axis=-1, keepdims=True)
+            local_out[b, odd] = jnp.dot(
+                weights[odd, :, pl.ds(0, tokens)], val[pl.ds(0, tokens)],
+                preferred_element_type=F32,
+            )
+        return carry
+
+    lax.fori_loop(0, blocks, own_keys, 0)
+
+    def rise(d, carry):
+        pl.semaphore_wait(aware.at[d], 1)
+        second(d - z).start()
+        return carry
+
+    lax.fori_loop(z + 1, nz, rise, 0)
+
     total = part[...].astype(F32)
     for k in range(1, nz):
         second(k).wait_recv()
         total = total + got[1, k].astype(F32)
     around[...] = total.astype(BF16)
-    for k in row_order(row):
-        third(k).start()
+    to_row(third)
     kv_all[pl.ds(pl.multiple_of(tokens + r * KB, KB), KB)] = total.astype(BF16)
     wo_in.wait()
     for k in range(1, row):
@@ -219,85 +288,117 @@
         at = pl.multiple_of(lax.rem(s + shift, ntp) * cols, cols)
         return wo[:, pl.ds(at, cols)]
 
-    def attend(b):
+    count = NHOT * KB
+    stacked = q_even.shape[1]
+
+    def hot_scores(b):
+        for odd, q, rhs, val in sides:
+            both_q = q[pl.ds(b, 2)].reshape(2 * stacked, 2 * HD)
+            hot_sc[odd] = lax.dot_general(
+                both_q, rhs[pl.ds(tokens, count)], (((1,), (1,)), ((), ())),
+                preferred_element_type=F32,
+            )
+
+    def attend(b, n):
         outs = []
-        for odd, q, rhs, val in ((0, q_even, kv_all, vk_all), (1, q_odd, vk_all, kv_all)):
-            scores[odd] = lax.dot_general(
-                q[b], rhs[...], (((1,), (1,)), ((), ())), preferred_element_type=F32
+        for odd, q, rhs, val in sides:
+            kept, norms = [], []
+            for i, p in strips:
+                rows = pl.ds(i * QB + p * quarter, quarter)
+                factor = scale[2 * i + odd] * (HD ** (-0.5) * LOG2E)
+                seen = bias[b, pl.ds(p * quarter, quarter), pl.ds(tokens, count)]
+                at = n * stacked + i * QB + p * quarter
+                sc = hot_sc[odd, pl.ds(at, quarter)] * factor + seen
+                before = local_top[b, odd, rows]
+                top = jnp.maximum(before, jnp.max(sc, axis=-1, keepdims=True))
+                lifted = jnp.exp2(sc - top)
+                hot_w[n, odd, rows] = lifted.astype(BF16)
+                fade = jnp.exp2(before - top)
+                norm = 1.0 / (fade * local_sum[b, odd, rows] + jnp.sum(lifted, axis=-1, keepdims=True))
+                kept.append(fade * norm)
+                norms.append(norm)
+            fresh = jnp.dot(
+                hot_w[n, odd], val[pl.ds(tokens, count)], preferred_element_type=F32
             )
-            for i in range(pairs):
-                factor = scale[2 * i + odd] * HD ** (-0.5)
-                for p in range(2):
-                    rows = pl.ds(i * QB + p * (QB // 2), QB // 2)
-                    sc = scores[odd, rows] * factor + bias[b, pl.ds(p * (QB // 2), QB // 2)]
-                    top = jnp.max(sc, axis=-1, keepdims=True)
-                    lifted = jnp.exp(sc - top)
-                    norm = 1.0 / jnp.sum(lifted, axis=-1, keepdims=True)
-                    weights[odd, rows] = (lifted * norm).astype(BF16)
-            outs.append(jnp.dot(weights[odd], val[...], preferred_element_type=F32))
-        tiles = [
-            jnp.where(low, outs[0][i * QB : (i + 1) * QB], outs[1][i * QB : (i + 1) * QB])
+            tiles = []
+            for m, (i, p) in enumerate(strips):
+                at = i * QB + p * quarter
+                tiles.append(
+                    local_out[b, odd, pl.ds(at, quarter)] * kept[m]
+                    + fresh[at : at + quarter] * norms[m]
+                )
+            outs.append(tiles)
+        half_low = low[:quarter]
+        heads = [
+            jnp.concatenate(
+                [jnp.where(half_low, outs[0][2 * i + p], outs[1][2 * i + p]) for p in range(2)],
+                axis=0,
+            )
             for i in range(pairs)
         ]
-        return jnp.concatenate(tiles, axis=1).astype(BF16)
-
-    def produce(c):
-        att = attend(c)
-        far = jnp.dot(att, columns(2), preferred_element_type=F32).astype(BF16)
-        opp[c, 0] = far[:, :half]
-        opp[c, 1] = far[:, half:]
-        copy(0, c).start()
-        copy(1, c).start()
-        to_left = jnp.dot(att, columns(ntp - 1), preferred_element_type=F32).astype(BF16)
-        side[c, 0, 0] = to_left[:, :half]
-        side[c, 0, 1] = to_left[:, half:]
-        copy(2, c).start()
-        to_right = jnp.dot(att, columns(1), preferred_element_type=F32).astype(BF16)
-        side[c, 1, 0] = to_right[:, :half]
-        side[c, 1, 1] = to_right[:, half:]
-        copy(3, c).start()
-        own[c] = jnp.dot(att, columns(0), preferred_element_type=F32).astype(BF16)
-
-    def combine(c):
+        return jnp.concatenate(heads, axis=1).astype(BF16)
+
+    def combine(c, carry):
         for d in range(2):
             copy(d, c).wait_recv()
             side[c, d, d] = (side[c, d, d].astype(F32) + via[c, d].astype(F32)).astype(BF16)
             copy(4 + d, c).start()
-
-    def finish(c):
+        return carry
+
+    def finish(c, carry):
         for kind in range(2, 6):
             copy(kind, c).wait_recv()
+        for kind in range(6):
+            copy(kind, c).wait_send()
         rows = pl.ds(pl.multiple_of(c * QB, QB), QB)
         for h in range(2):
             part_sum = own[c, :, h * half : (h + 1) * half].astype(F32)
             part_sum = part_sum + arrived[c, 0, h].astype(F32) + arrived[c, 1, h].astype(F32)
             out_ref[rows, h * half : (h + 1) * half] = part_sum.astype(BF16)
-
-    def step(c, carry):
-        @pl.when(c < blocks)
+        return carry
+
+    def product(att, shift):
+        return jnp.dot(att, columns(shift), preferred_element_type=F32).astype(BF16)
+
+    def produce(g, carry):
+        hot_scores(2 * g)
+        atts = []
+        for n in range(2):
+            c = 2 * g + n
+            att = attend(c, n)
+            atts.append(att)
+            far = product(att, 2)
+            opp[c, 0] = far[:, :half]
+            opp[c, 1] = far[:, half:]
+            copy(0, c).start()
+            copy(1, c).start()
+        att = jnp.concatenate(atts, axis=0)
+        attended[pl.ds(pl.multiple_of(g * 2 * QB, 2 * QB), 2 * QB)] = att
+        for d, shift in ((0, ntp - 1), (1, 1)):
+            beside = product(att, shift)
+            for n in range(2):
+                part_rows = beside[n * QB : (n + 1) * QB]
+                side[2 * g + n, d, 0] = part_rows[:, :half]
+                side[2 * g + n, d, 1] = part_rows[:, half:]
+                copy(2 + d, 2 * g + n).start()
+
+        @pl.when(g > 0)
         def _():
-            produce(c)
-
-        @pl.when((c >= 1) & (c <= blocks))
-        def _():
-            combine(c - 1)
-
-        @pl.when(c >= 2)
-        def _():
-            finish(c - 2)
-
-        return carry
-
-    lax.fori_loop(0, blocks + 2, step, 0)
-
+            for n in range(2):
+                combine(2 * g - 2 + n, 0)
+
+        return carry
+
+    lax.fori_loop(0, blocks // 2, produce, 0)
+    own[...] = product(attended[...], 0).reshape(blocks, QB, cols)
+    for n in range(2):
+        combine(blocks - 2 + n, 0)
     for k in range(1, row):
         first(k).wait_send()
         third(k).wait_send()
     for k in range(1, nz):
         second(k).wait_send()
-    for c in range(blocks):
-        for kind in range(6):
-            copy(kind, c).wait_send()
+    lax.fori_loop(0, blocks, finish, 0)
 
 
 def local(
@@ -324,13 +425,13 @@
     anywhere = pl.BlockSpec(memory_space=pl.ANY)
     return pl.pallas_call(
         functools.partial(kernel, dims),
-        out_shape=jax.ShapeDtypeStruct((tokens, cols), BF16),
+        out_shape=pltpu.VMEM((tokens, cols), BF16),
         in_specs=[anywhere] * 8,
         out_specs=pl.BlockSpec(memory_space=pltpu.VMEM),
         scratch_shapes=[
             pltpu.VMEM((tokens, width), BF16),
             pltpu.VMEM((width, head_cols), BF16),
-            pltpu.VMEM((4 * HD, width), BF16),
+            pltpu.VMEM((2 * HD, width), BF16),
             pltpu.VMEM((head_cols, out_cols), BF16),
             pltpu.SMEM((head_cols // HD,), F32),
             pltpu.SMEM((NHOT,), jnp.int32),
@@ -345,18 +446,25 @@
             pltpu.VMEM((2, NHOT, KB, 2 * HD), BF16),
             pltpu.VMEM((KB, 2 * HD), BF16),
             pltpu.VMEM((KB, 2 * HD), BF16),
-            pltpu.VMEM((2, stacked, keys), F32),
-            pltpu.VMEM((2, stacked, keys), BF16),
+            pltpu.VMEM((2, stacked, tokens), F32),
+            pltpu.VMEM((2, stacked, tokens), BF16),
+            pltpu.VMEM((blocks, 2, stacked, 2 * HD), F32),
+            pltpu.VMEM((blocks, 2, stacked, 1), F32),
+            pltpu.VMEM((blocks, 2, stacked, 1), F32),
+            pltpu.VMEM((2, 2 * stacked, NHOT * KB), F32),
+            pltpu.VMEM((2, 2, stacked, NHOT * KB), BF16),
+            pltpu.VMEM((tokens, head_cols), BF16),
             pltpu.VMEM((blocks, 2, QB, half), BF16),
             pltpu.VMEM((blocks, 2, QB, half), BF16),
             pltpu.VMEM((blocks, 2, 2, QB, half), BF16),
             pltpu.VMEM((blocks, 2, 2, QB, half), BF16),
             pltpu.VMEM((blocks, QB, cols), BF16),
-            pltpu.SemaphoreType.DMA((10,)),
+            pltpu.SemaphoreType.DMA((7 + PIECES,)),
             pltpu.SemaphoreType.DMA((3, NHOT)),
             pltpu.SemaphoreType.DMA((3, NHOT)),
             pltpu.SemaphoreType.DMA((6, blocks)),
             pltpu.SemaphoreType.DMA((6, blocks)),
+            pltpu.SemaphoreType.REGULAR((16,)),
         ],
         compiler_params=pltpu.CompilerParams(collective_id=0, has_side_effects=True),
     )(

time: 69.1 us -> 60.3 us (0.87)
  the two profiles are of different devices: /device:TPU:8 before, /device:TPU:1 now
where the time goes in v2:
time: 60.3 us; the launch traced here: 60.1 us
  Pallas kernels  59.4 us (99%)
  local copies, waits for them, and re-layouts  0.75 us (1%)
    pallas_call x1, Pallas kernels, local(): pl.pallas_call(functools.partial(kernel, dims), out_shape=pltpu.VMEM((tok...  59.4 us

profile of v2, /device:TPU:1, one launch (start us, length us, event | category | flops | bytes accessed | tf_op | source)
XLA Modules:
  0.0 60.1 jit_solution(15665440403467484059)
XLA Ops:
  0.0 59.4 %shard_map.82 = bf16[384,512]{1,0:T(8,128)(2,1)S(1)} custom-call(bf16[384,2048]{1,0:T(8,128)(2,1)} %x_hbm.1, bf16[2048,512]{1,0:T(8,128)(2,1)} %wq_hbm.1, bf16[64,2048]{1,0:T(8,128)(2,1)} %bitcast.2, bf16[64,2048]{1,0:T(8,128)(2,1)} %bitcast.3, bf16[512,2048]{1,0:T(8,128)(2,1)} %wo_hbm.1, f32[8]{0:T(128)} %scale_hbm.1, s32[16]{0:T(128)} %hot_hbm.1, ...), custom_call_target="tpu_custom_call" | custom-call | tf_op jit(solution)/shard_map/pallas_call | solution.py:426
  59.4 0.7 %copy.10 = bf16[384,512]{1,0:T(8,128)(2,1)} copy(bf16[384,512]{1,0:T(8,128)(2,1)S(1)} %shard_map.82) | data formatting | bytes 786432

commit v3 on v2

--- a/solution.py
+++ b/solution.py
@@ -15,6 +15,7 @@
 NHOT = 16
 FAR = 1 << 30
 PIECES = 4
+GROUP = 4
 LOG2E = 1.4426950408889634
 F32 = jnp.float32
 BF16 = jnp.bfloat16
@@ -155,6 +156,12 @@
             device_id=in_z(k), device_id_type=MESH,
         )
 
+    def passed(k):
+        return pltpu.make_async_remote_copy(
+            around, got.at[1, k], hot_send.at[1, k], hot_recv.at[1, k],
+            device_id=in_z(k), device_id_type=MESH,
+        )
+
     def third(k):
         rows = pl.ds(pl.multiple_of(tokens + r * KB, KB), KB)
         return pltpu.make_async_remote_copy(
@@ -172,7 +179,15 @@
         pl.semaphore_signal(aware.at[z], inc=1, device_id={"z": d}, device_id_type=MESH)
         return carry
 
-    lax.fori_loop(0, z, below, 0)
+    member = lax.rem(z, GROUP)
+
+    @pl.when(member == 0)
+    def _():
+        lax.fori_loop(0, z, below, 0)
+
+    @pl.when(member > 0)
+    def _():
+        below(z - member, 0)
     kv_all[pl.ds(0, tokens)] = packed
     vk_all[pl.ds(0, tokens)] = pltpu.roll(packed.astype(F32), HD, 1).astype(BF16)
 
@@ -192,11 +207,11 @@
         total = total + got[0, k].astype(F32)
     part[...] = total.astype(BF16)
 
-    def sink(d, carry):
-        second(lax.rem(d - z + nz, nz)).start()
-        return carry
-
-    lax.fori_loop(0, z, sink, 0)
+    def sink(g, carry):
+        second(lax.rem(g * GROUP - z + nz, nz)).start()
+        return carry
+
+    lax.fori_loop(0, (z + GROUP - 1) // GROUP, sink, 0)
 
     codes_in.wait()
     scale_in.wait()
@@ -247,20 +262,31 @@
 
     lax.fori_loop(0, blocks, own_keys, 0)
 
-    def rise(d, carry):
-        pl.semaphore_wait(aware.at[d], 1)
-        second(d - z).start()
-        return carry
-
-    lax.fori_loop(z + 1, nz, rise, 0)
-
-    total = part[...].astype(F32)
-    for k in range(1, nz):
-        second(k).wait_recv()
-        total = total + got[1, k].astype(F32)
-    around[...] = total.astype(BF16)
+    def rise(g, carry):
+        pl.semaphore_wait(aware.at[g * GROUP], 1)
+        second(g * GROUP - z).start()
+        return carry
+
+    lax.fori_loop(z // GROUP + 1, nz // GROUP, rise, 0)
+
+    @pl.when(member == 0)
+    def _():
+        whole = part[...].astype(F32)
+        for k in range(1, nz):
+            second(k).wait_recv()
+            whole = whole + got[1, k].astype(F32)
+        around[...] = whole.astype(BF16)
+        for k in range(1, GROUP):
+            pl.semaphore_wait(aware.at[z + k], 1)
+            passed(k).start()
+
+    @pl.when(member > 0)
+    def _():
+        passed(member).wait_recv()
+        around[...] = got[1, member]
+
     to_row(third)
-    kv_all[pl.ds(pl.multiple_of(tokens + r * KB, KB), KB)] = total.astype(BF16)
+    kv_all[pl.ds(pl.multiple_of(tokens + r * KB, KB), KB)] = around[...]
     wo_in.wait()
     for k in range(1, row):
         third(k).wait_recv()
@@ -396,8 +422,17 @@
     for k in range(1, row):
         first(k).wait_send()
         third(k).wait_send()
-    for k in range(1, nz):
-        second(k).wait_send()
+    for g in range(nz // GROUP):
+
+        @pl.when(g * GROUP != z)
+        def _():
+            second(lax.rem(g * GROUP - z + nz, nz)).wait_send()
+
+    @pl.when(member == 0)
+    def _():
+        for k in range(1, GROUP):
+            passed(k).wait_send()
+
     lax.fori_loop(0, blocks, finish, 0)
 
 

time: 60.3 us -> 57.9 us (0.960)
  Pallas kernels: 59.4 us -> 56.6 us
    pallas_call x1, Pallas kernels: 59.4 us -> 56.6 us  [local(): pl.pallas_call(functools.partial(kernel, dims), out_shape=pltpu.VMEM((tok...]
where the time goes in v3:
time: 57.9 us; the launch traced here: 57.3 us
  Pallas kernels  56.6 us (98%)
  local copies, waits for them, and re-layouts  0.75 us (1%)
    pallas_call x1, Pallas kernels, local(): pl.pallas_call(functools.partial(kernel, dims), out_shape=pltpu.VMEM((tok...  56.6 us

profile of v3, /device:TPU:1, one launch (start us, length us, event | category | flops | bytes accessed | tf_op | source)
XLA Modules:
  0.0 57.3 jit_solution(9930095725373149973)
XLA Ops:
  0.0 56.6 %shard_map.82 = bf16[384,512]{1,0:T(8,128)(2,1)S(1)} custom-call(bf16[384,2048]{1,0:T(8,128)(2,1)} %x_hbm.1, bf16[2048,512]{1,0:T(8,128)(2,1)} %wq_hbm.1, bf16[64,2048]{1,0:T(8,128)(2,1)} %bitcast.2, bf16[64,2048]{1,0:T(8,128)(2,1)} %bitcast.3, bf16[512,2048]{1,0:T(8,128)(2,1)} %wo_hbm.1, f32[8]{0:T(128)} %scale_hbm.1, s32[16]{0:T(128)} %hot_hbm.1, ...), custom_call_target="tpu_custom_call" | custom-call | tf_op jit(solution)/shard_map/pallas_call | solution.py:461
  56.6 0.7 %copy.10 = bf16[384,512]{1,0:T(8,128)(2,1)} copy(bf16[384,512]{1,0:T(8,128)(2,1)S(1)} %shard_map.82) | data formatting | bytes 786432
